TPU v7x, 32 devices: a whole 2x2x4 slice. The times are simulated.
32 devices in a mesh: sp: 16 (over z, y, x), tp: 2 (over core).
Axes of the slice: x: 2, y: 2, z: 4, core: 2. Of those that a mesh axis runs over, the one named last changes fastest.
Arguments:
- x_rows: bfloat16 [2048, 2048], P('sp'), may hold values from -6 to 6
- queries: bfloat16 [2048, 1024], P('sp', 'tp'), may hold values from -8 to 8
- keys: bfloat16 [2048, 512], P('sp', 'tp'), may hold values from -8 to 8
- values: bfloat16 [2048, 512], P('sp', 'tp'), may hold values from -6 to 6
- query_norm_gain: float32 [64], replicated, may hold values from 1 to 8
- key_norm_gain: float32 [64], replicated, may hold values from 1 to 8
- out_weight: bfloat16 [1024, 2048], P('tp'), may hold values from -0.1875 to 0.1875
- ffn_gain: float32 [2048], replicated, may hold values from 0.1 to 1.9
- gate_weight: bfloat16 [2048, 5120], P('sp', 'tp'), may hold values from -0.125 to 0.125
- value_weight: bfloat16 [2048, 5120], P('sp', 'tp'), may hold values from -0.125 to 0.125
- conv_gate: float32 [3, 5120], P(None, 'tp'), may hold values from -3.5 to 3.5
- conv_value: float32 [3, 5120], P(None, 'tp'), may hold values from -3.5 to 3.5
- down_weight: bfloat16 [2048, 5120], P('sp', 'tp'), may hold values from -0.078125 to 0.078125
Outputs:
- layer_out: bfloat16 [2048, 2048], P('sp')
All inputs are finite; a program needn't handle non-finite values.
Results may differ from a plain program's by a relative error of at most 0.017.
Values may be sent and summed in bfloat16 or wider, within the bound.
A program may use at most 64 MiB of HBM per device.

v0:
```python
import math
import jax
import jax.numpy as jnp
from jax import lax
from jax.sharding import PartitionSpec as P

HEAD_SIZE = 64
GRID_ROW_WIDTH = 64
eps_norm = 1e-06
theta = 10000.0


def with_halo(cells, sides, width):
    for axis, dim in sides:
        count = lax.axis_size(axis)
        ends = count - 1
        head = lax.slice_in_dim(cells, 0, width, axis=dim)
        tail = lax.slice_in_dim(cells, cells.shape[dim] - width, cells.shape[dim], axis=dim)
        cells = jnp.concatenate(
            [
                lax.ppermute(tail, axis, [(i, (i + 1) % count) for i in range(ends)]),
                cells,
                lax.ppermute(head, axis, [((i + 1) % count, i) for i in range(ends)]),
            ],
            axis=dim,
        )
    return cells


def per_head_norm(head_block, gain_vec):
    wide_vals = head_block.astype(jnp.float32)
    inverse_rms = lax.rsqrt(jnp.mean(wide_vals * wide_vals, axis=-1, keepdims=True) + eps_norm)
    return wide_vals * inverse_rms * gain_vec


def turn_half(half_vec, places):
    quarter_len = half_vec.shape[-1] // 2
    inverse_rates = 1.0 / theta ** (
        jnp.arange(quarter_len, dtype=jnp.float32) * 2.0 / half_vec.shape[-1]
    )
    angles = places.astype(jnp.float32)[:, None] * inverse_rates[None, :]
    angles = jnp.concatenate([angles, angles], axis=-1)[:, None, :]
    front_part = half_vec[..., :quarter_len]
    back_part = half_vec[..., quarter_len:]
    return half_vec * jnp.cos(angles) + jnp.concatenate(
        [-back_part, front_part], axis=-1
    ) * jnp.sin(angles)


def apply_rotary(normed_heads, token_positions):
    half_point = normed_heads.shape[-1] // 2
    grid_row = token_positions // GRID_ROW_WIDTH
    grid_col = token_positions % GRID_ROW_WIDTH
    return jnp.concatenate(
        [
            turn_half(normed_heads[..., :half_point], grid_row),
            turn_half(normed_heads[..., half_point:], grid_col),
        ],
        axis=-1,
    )


def row_norm(rows_wide, gain_vec):
    inverse_rms = lax.rsqrt(jnp.mean(rows_wide * rows_wide, axis=-1, keepdims=True) + eps_norm)
    return (rows_wide * inverse_rms * gain_vec).astype(jnp.bfloat16)


def contract_units(left_rows, right_rows):
    return lax.dot_general(
        left_rows, right_rows, (((1,), (1,)), ((), ())), preferred_element_type=jnp.float32
    )


def shards(
    x_rows,
    queries,
    keys,
    values,
    query_norm_gain,
    key_norm_gain,
    out_weight,
    ffn_gain,
    gate_weight,
    value_weight,
    conv_gate,
    conv_value,
    down_weight,
):
    collected = (
        lax.all_gather(gate_weight, "sp", axis=0, tiled=True),
        lax.all_gather(value_weight, "sp", axis=0, tiled=True),
        lax.all_gather(down_weight, "sp", axis=0, tiled=True),
    )
    tokens_here = queries.shape[0]
    query_heads = queries.shape[1] // HEAD_SIZE
    key_heads = keys.shape[1] // HEAD_SIZE
    group_width = query_heads // key_heads
    lane_rows = group_width * tokens_here
    token_positions = lax.axis_index("sp") * tokens_here + jnp.arange(tokens_here, dtype=jnp.int32)
    rotated_queries = apply_rotary(
        per_head_norm(queries.reshape(tokens_here, query_heads, HEAD_SIZE), query_norm_gain),
        token_positions,
    )
    query_lanes = rotated_queries.reshape(tokens_here, key_heads, group_width, HEAD_SIZE).transpose(
        1, 2, 0, 3
    )
    query_lanes = query_lanes.reshape(key_heads, lane_rows, HEAD_SIZE) * HEAD_SIZE ** (-0.5)
    start_state = (
        jnp.full((key_heads, lane_rows), -1e30, jnp.float32),
        jnp.zeros((key_heads, lane_rows), jnp.float32),
        jnp.zeros((key_heads, lane_rows, HEAD_SIZE), jnp.float32),
    )
    key_piece = lax.all_gather(keys, "sp", axis=0, tiled=True)
    value_piece = lax.all_gather(values, "sp", axis=0, tiled=True)
    row_count = key_piece.shape[0]
    key_places = jnp.arange(row_count, dtype=jnp.int32)
    turned = apply_rotary(
        per_head_norm(key_piece.reshape(row_count, key_heads, HEAD_SIZE), key_norm_gain), key_places
    )
    key_span = math.gcd(row_count, 2048)
    span_count = row_count // key_span
    turned = turned.reshape(span_count, key_span, key_heads, HEAD_SIZE)
    value_matrix = value_piece.reshape(span_count, key_span, key_heads, HEAD_SIZE)

    def one_span(state_now, inputs):
        running_top, denominator, weighted = state_now
        key_block, value_block = inputs
        scores = jnp.einsum("hrd,shd->hrs", query_lanes, key_block, precision=lax.Precision.HIGHEST)
        new_top = jnp.maximum(running_top, jnp.max(scores, axis=-1))
        factor = jnp.exp(running_top - new_top)
        weights = jnp.exp(scores - new_top[..., None])
        denominator = denominator * factor + jnp.sum(weights, axis=-1)
        weighted = weighted * factor[..., None] + jnp.einsum(
            "hrs,shd->hrd",
            weights.astype(jnp.bfloat16),
            value_block,
            preferred_element_type=jnp.float32,
        )
        return ((new_top, denominator, weighted), None)

    folded_state, _ = lax.scan(one_span, start_state, (turned, value_matrix))
    running_top, denominator, weighted = folded_state
    attended = (weighted / denominator[..., None]).reshape(
        key_heads, group_width, tokens_here, HEAD_SIZE
    )
    attended = (
        attended.transpose(2, 0, 1, 3)
        .reshape(tokens_here, query_heads * HEAD_SIZE)
        .astype(jnp.bfloat16)
    )
    share_rows = tokens_here // lax.axis_size("tp")
    head_share = lax.psum_scatter(
        jnp.dot(attended, out_weight, preferred_element_type=jnp.float32).astype(jnp.bfloat16),
        "tp",
        scatter_dimension=0,
        tiled=True,
    ).astype(jnp.float32)
    own_rows = lax.dynamic_slice_in_dim(x_rows, lax.axis_index("tp") * share_rows, share_rows, 0)
    middle_rows = own_rows.astype(jnp.float32) + head_share
    normed = lax.all_gather(row_norm(middle_rows, ffn_gain), "tp", axis=0, tiled=True)
    unit_local = gate_weight.shape[1]
    gate_pre = jnp.dot(normed, collected[0], preferred_element_type=jnp.float32).astype(
        jnp.bfloat16
    )
    value_pre = jnp.dot(normed, collected[1], preferred_element_type=jnp.float32).astype(
        jnp.bfloat16
    )
    joined = jnp.concatenate([gate_pre, value_pre], axis=1)
    padded = with_halo(joined, (("sp", 0),), 1).astype(jnp.float32)
    conv_taps = jnp.concatenate([conv_gate, conv_value], axis=1)
    convolved = conv_taps[0] * padded[:-2] + conv_taps[1] * padded[1:-1] + conv_taps[2] * padded[2:]
    hidden = (jax.nn.silu(convolved[:, :unit_local]) * convolved[:, unit_local:]).astype(
        jnp.bfloat16
    )
    unit_share = lax.psum_scatter(
        contract_units(hidden, collected[2]).astype(jnp.bfloat16),
        "tp",
        scatter_dimension=0,
        tiled=True,
    ).astype(jnp.float32)
    finished = (middle_rows + unit_share).astype(jnp.bfloat16)
    return lax.all_gather(finished, "tp", axis=0, tiled=True)


def solution(mesh):
    placed = (
        P("sp", None),
        P("sp", "tp"),
        P("sp", "tp"),
        P("sp", "tp"),
        P(),
        P(),
        P("tp", None),
        P(),
        P("sp", "tp"),
        P("sp", "tp"),
        P(None, "tp"),
        P(None, "tp"),
        P("sp", "tp"),
    )
    return jax.shard_map(
        shards, mesh=mesh, in_specs=placed, out_specs=P("sp", None), check_vma=False
    )
```

profile of v0, /device:TPU:0, one launch (start us, length us, event | category | flops | bytes accessed | tf_op | source)
XLA Modules:
  0.0 565.5 jit_solution(3756514513751878015)
XLA Ops:
  10.3 1.9 fusion.33
  12.2 55.7 %all-gather.6.cloned.1.call-done = bf16[2048,256]{1,0:T(8,128)(2,1)} async-done(((bf16[128,256]{1,0:T(8,128)(2,1)}), bf16[2048,256]{1,0:T(8,128)(2,1)}) %all-gather.6.cloned.1.call-update) | async-done | bytes 1048592 | tf_op jit(solution)/shard_map/all_gather | solution.py:113
  67.9 2.6 copy.18
  70.5 2.0 multiply_reduce_fusion
  73.9 7.3 %fusion.57 = (f32[4,256]{1,0:T(4,128)S(1)}, f32[4,256,2048]{2,1,0:T(8,128)S(1)}) fusion(f32[2048,4,32]{0,2,1:T(8,128)S(1)} %get-tuple-element.18, f32[2048,4,32]{0,2,1:T(8,128)S(1)} %get-tuple-element.17, f32[4,2,8,8,128]{4,3,2,1,0:T(8,128)S(1)} %bitcast.37), kind=kOutput, calls=%fused_computation.107 | convolution fusion | flops 1613233152 | bytes 10752000 | tf_op jit(solution)/shard_map/while/body/eval_jaxpr/hrd,shd->hrs/dot_general | solution.py:128
  81.3 1.3 fusion
  82.6 2.0 copy-done.2
  84.5 40.1 %all-gather.8.cloned.1.call-done = bf16[2048,256]{1,0:T(8,128)(2,1)} async-done(((bf16[128,256]{1,0:T(8,128)(2,1)}), bf16[2048,256]{1,0:T(8,128)(2,1)}) %all-gather.8.cloned.1.call-update) | async-done | bytes 1048592 | tf_op jit(solution)/shard_map/all_gather | solution.py:114
  124.6 1.7 copy.19
  126.3 4.9 fusion.21
  134.4 5.0 reduce-scatter.3.cloned.1.call-done
  141.7 2.2 all_gather.23
  143.9 130.8 %all-gather.12.cloned.1.call-done = bf16[2048,2560]{1,0:T(8,128)(2,1)} async-done(((bf16[128,2560]{1,0:T(8,128)(2,1)}), bf16[2048,2560]{1,0:T(8,128)(2,1)}) %all-gather.12.cloned.1.call-update) | async-done | bytes 10485776 | tf_op jit(solution)/shard_map/all_gather | solution.py:91
  274.6 5.5 convolution_convert_fusion
  280.2 126.7 %all-gather.10.cloned.1.call-done = bf16[2048,2560]{1,0:T(8,128)(2,1)} async-done(((bf16[128,2560]{1,0:T(8,128)(2,1)}), bf16[2048,2560]{1,0:T(8,128)(2,1)}) %all-gather.10.cloned.1.call-update) | async-done | bytes 10485776 | tf_op jit(solution)/shard_map/all_gather | solution.py:90
  406.9 5.5 convolution_convert_fusion.1
  412.4 3.4 collective-permute-start
  415.8 1.3 collective-permute-start.1
  417.4 4.6 collective-permute-done.1
  422.4 2.3 fusion.5
  424.7 114.3 %all-gather.14.cloned.1.call-done = bf16[2048,2560]{1,0:T(8,128)(2,1)} async-done(((bf16[128,2560]{1,0:T(8,128)(2,1)}), bf16[2048,2560]{1,0:T(8,128)(2,1)}) %all-gather.14.cloned.1.call-update) | async-done | bytes 10485776 | tf_op jit(solution)/shard_map/all_gather | solution.py:92
  539.1 9.2 %convolution_convert_fusion.3 = bf16[128,2048]{1,0:T(8,128)(2,1)} fusion(bf16[2048,2560]{1,0:T(8,128)(2,1)} %all-gather.14.cloned.1.call-done, f32[128,5120]{1,0:T(8,128)} %fusion.5), kind=kOutput, calls=%fused_computation.13 | convolution fusion | flops 1344405504 | bytes 13631488 | tf_op jit(solution)/shard_map/dot_general | solution.py:69
  548.3 6.3 %reduce-scatter.5.cloned.1.call-done = bf16[64,2048]{1,0:T(8,128)(2,1)} async-done(((bf16[128,2048]{1,0:T(8,128)(2,1)}), bf16[64,2048]{1,0:T(8,128)(2,1)}) %reduce-scatter.5.cloned.1.call-update) | async-done | bytes 262160 | tf_op jit(solution)/shard_map/reduce_scatter | solution.py:175
  555.6 2.2 all_gather.27
  (67 shorter events, 13.0 us)
Async XLA Ops:
  6.5 124.7 %copy-start = (bf16[512,2048]{1,0:T(8,128)(2,1)S(1)}, bf16[512,2048]{1,0:T(8,128)(2,1)}, u32[]{:S(2)}) copy-start(bf16[512,2048]{1,0:T(8,128)(2,1)} %param.19) | copy-start | bytes 6291460
  6.5 61.4 %all-gather.6.cloned.1.call-start = ((), (), s32[]{:S(2)}) async-start(), calls=%async_computation.2 | async-start | bytes 1114112 | tf_op jit(solution)/shard_map/all_gather | solution.py:113
  7.3 117.4 %all-gather.8.cloned.1.call-start = ((), (), s32[]{:S(2)}) async-start(), calls=%async_computation.3 | async-start | bytes 1114112 | tf_op jit(solution)/shard_map/all_gather | solution.py:114
  8.0 131.5 %reduce-scatter.3.cloned.1.call-start = ((), (), s32[]{:S(2)}) async-start(), calls=%async_computation.4 | async-start | bytes 786432 | tf_op jit(solution)/shard_map/reduce_scatter | solution.py:152
  12.2 60.3 %copy-start.9 = (f32[64]{0:T(128)S(1)}, f32[64]{0:T(128)}, u32[]{:S(2)}) copy-start(f32[64]{0:T(128)} %param.18) | copy-start | bytes 772
  70.5 2.2 copy-start.3
  81.3 3.3 copy-start.2
  131.2 3.1 copy-start.6
  131.2 3.2 copy-start.7
  131.2 8.2 %copy-start.5 = (bf16[128,2048]{1,0:T(8,128)(2,1)S(1)}, bf16[128,2048]{1,0:T(8,128)(2,1)}, u32[]{:S(2)}) copy-start(bf16[128,2048]{1,0:T(8,128)(2,1)} %param.13) | copy-start | bytes 1572868
  131.3 9.4 %copy-start.8 = (f32[2048]{0:T(1024)S(1)}, f32[2048]{0:T(1024)}, u32[]{:S(2)}) copy-start(f32[2048]{0:T(1024)} %param.20) | copy-start | bytes 24580
  132.6 142.1 %all-gather.12.cloned.1.call-start = ((), (), s32[]{:S(2)}) async-start(), calls=%async_computation.6 | async-start | bytes 11141120 | tf_op jit(solution)/shard_map/all_gather | solution.py:91
  133.1 273.7 %all-gather.10.cloned.1.call-start = ((), (), s32[]{:S(2)}) async-start(), calls=%async_computation.5 | async-start | bytes 11141120 | tf_op jit(solution)/shard_map/all_gather | solution.py:90
  133.7 405.4 %all-gather.14.cloned.1.call-start = ((), (), s32[]{:S(2)}) async-start(), calls=%async_computation.7 | async-start | bytes 11141120 | tf_op jit(solution)/shard_map/all_gather | solution.py:92
  134.3 420.3 %reduce-scatter.5.cloned.1.call-start = ((), (), s32[]{:S(2)}) async-start(), calls=%async_computation.8 | async-start | bytes 786432 | tf_op jit(solution)/shard_map/reduce_scatter | solution.py:175
  412.4 5.0 collective-permute-start
  415.8 6.2 %collective-permute-start.1 = (bf16[1,5120]{1,0:T(2,128)(2,1)S(1)}, bf16[1,5120]{1,0:T(2,128)(2,1)S(1)}, u32[]{:S(2)}, u32[]{:S(2)}) collective-permute-start(bf16[1,5120]{1,0:T(2,128)(2,1)S(1)} %get-tuple-element.33), channel_id=1, source_target_pairs={{2,0},{4,2},{6,4},{8,6},{10,8},{12,10},{14,12},{16,14},{18,16},{20... | collective-permute-start | bytes 30728 | tf_op jit(solution)/shard_map/ppermute | solution.py:23
  424.7 129.8 %copy-start.4 = (bf16[64,2048]{1,0:T(8,128)(2,1)S(1)}, bf16[64,2048]{1,0:T(8,128)(2,1)}, u32[]{:S(2)}) copy-start(bf16[64,2048]{1,0:T(8,128)(2,1)} %reduce-scatter.3.cloned.1.call-done) | copy-start | bytes 786436
  539.1 19.5 %copy-start.1 = (bf16[512,2048]{1,0:T(8,128)(2,1)S(1)}, bf16[512,2048]{1,0:T(8,128)(2,1)}, u32[]{:S(2)}) copy-start(bf16[512,2048]{1,0:T(8,128)(2,1)} %param.19) | copy-start | bytes 6291460
Sparse Core Ops, SparseCore 0:
  10.1 57.7 all-gather.5
  70.7 53.9 all-gather.7
  132.7 6.7 reduce-scatter.2
  142.0 132.5 all-gather.11
  277.2 129.6 all-gather.9
  409.4 129.6 all-gather.13
  548.4 6.0 reduce-scatter.4
where the time goes:
time: 566 us; the launch traced here: 565 us
  waiting for transfers between devices  487 us (86%)
  matrix products  33.7 us (6%)
  between operations  13.8 us (2%)
  other arithmetic  13.5 us (2%)
  local copies, waits for them, and re-layouts  8.35 us (1%)
    all_gather x1, waiting for transfers between devices, shards(): lax.all_gather(value_weight, 'sp', axis=0, tiled=True)  131 us
    all_gather x1, waiting for transfers between devices, shards(): lax.all_gather(gate_weight, 'sp', axis=0, tiled=True)  127 us
    all_gather x1, waiting for transfers between devices, shards(): lax.all_gather(down_weight, 'sp', axis=0, tiled=True)  114 us
    all_gather x1, waiting for transfers between devices, shards(): key_piece = lax.all_gather(keys, 'sp', axis=0, tiled=True)  55.7 us
    all_gather x1, waiting for transfers between devices, shards(): value_piece = lax.all_gather(values, 'sp', axis=0, tiled=True)  40.1 us
  transfers between devices with their start and end apart: 9, of which 9 were waited for; matrix products, arithmetic and copies ran while one was open for 6% of the time, Pallas kernels for 0%

commit v1 on v0

--- a/solution.py
+++ b/solution.py
@@ -86,6 +86,23 @@
     conv_value,
     down_weight,
 ):
+
+    def _store_clusters(field_in, array_dim):
+        wide_n = lax.axis_size("sp")
+        column = [field_in]
+        for idx in range(wide_n - 1):
+            column.append(
+                lax.ppermute(
+                    column[-1], axis_name="sp", perm=[(q, (q + 1) % wide_n) for q in range(wide_n)]
+                )
+            )
+        tile_out = jnp.roll(
+            jnp.concatenate(column[::-1], array_dim),
+            (lax.axis_index("sp") + 1) * field_in.shape[array_dim],
+            array_dim,
+        )
+        return tile_out
+
     collected = (
         lax.all_gather(gate_weight, "sp", axis=0, tiled=True),
         lax.all_gather(value_weight, "sp", axis=0, tiled=True),
@@ -111,7 +128,7 @@
         jnp.zeros((key_heads, lane_rows, HEAD_SIZE), jnp.float32),
     )
     key_piece = lax.all_gather(keys, "sp", axis=0, tiled=True)
-    value_piece = lax.all_gather(values, "sp", axis=0, tiled=True)
+    value_piece = _store_clusters(values, 0)
     row_count = key_piece.shape[0]
     key_places = jnp.arange(row_count, dtype=jnp.int32)
     turned = apply_rotary(

time: 566 us -> 589 us (1.041)
  waiting for transfers between devices: 487 us -> 500 us
  local copies, waits for them, and re-layouts: 8.35 us -> 14.6 us
    ppermute x0 -> x15, waiting for transfers between devices: none -> 113 us  [_store_clusters(): lax.ppermute(column[-1], axis_name='sp', perm=[(q, (q + 1) % wide_n) for...]
    all_gather x1, waiting for transfers between devices: 55.7 us -> 0.02 us  [shards(): key_piece = lax.all_gather(keys, 'sp', axis=0, tiled=True)]
    all_gather x1 -> x0, waiting for transfers between devices: 40.1 us -> none  [shards(): value_piece = lax.all_gather(values, 'sp', axis=0, tiled=True)]
  transfers between devices with their start and end apart: 9 -> 23, of which waited for: 9 -> 22; matrix products, arithmetic and copies ran while one was open for 6% -> 5% of each run, Pallas kernels for 0% -> 0%
where the time goes in v1:
time: 589 us; the launch traced here: 588 us
  waiting for transfers between devices  500 us (85%)
  matrix products  30.4 us (5%)
  other arithmetic  16.6 us (3%)
  local copies, waits for them, and re-layouts  14.6 us (2%)
  between operations  14 us (2%)
  starting transfers between devices  8.11 us (1%)
    all_gather x1, waiting for transfers between devices, shards(): lax.all_gather(value_weight, 'sp', axis=0, tiled=True)  131 us
    all_gather x1, waiting for transfers between devices, shards(): lax.all_gather(gate_weight, 'sp', axis=0, tiled=True)  127 us
    all_gather x1, waiting for transfers between devices, shards(): lax.all_gather(down_weight, 'sp', axis=0, tiled=True)  114 us
    ppermute x15, waiting for transfers between devices, _store_clusters(): lax.ppermute(column[-1], axis_name='sp', perm=[(q, (q + 1) % wide_n) for...  113 us
  transfers between devices with their start and end apart: 23, of which 22 were waited for; matrix products, arithmetic and copies ran while one was open for 5% of the time, Pallas kernels for 0%

profile of v1, /device:TPU:0, one launch (start us, length us, event | category | flops | bytes accessed | tf_op | source)
XLA Modules:
  0.0 588.5 jit_solution(12251099008002264862)
XLA Ops:
  10.3 6.4 %collective-permute-done = bf16[128,256]{1,0:T(8,128)(2,1)S(1)} collective-permute-done((bf16[128,256]{1,0:T(8,128)(2,1)}, bf16[128,256]{1,0:T(8,128)(2,1)S(1)}, u32[]{:S(2)}, u32[]{:S(2)}) %collective-permute-start) | collective-permute-done | bytes 65568 | tf_op jit(solution)/shard_map/ppermute | solution.py:95
  16.8 7.9 %collective-permute-done.1 = bf16[128,256]{1,0:T(8,128)(2,1)S(1)} collective-permute-done((bf16[128,256]{1,0:T(8,128)(2,1)S(1)}, bf16[128,256]{1,0:T(8,128)(2,1)S(1)}, u32[]{:S(2)}, u32[]{:S(2)}) %collective-permute-start.1) | collective-permute-done | bytes 65568 | tf_op jit(solution)/shard_map/ppermute | solution.py:95
  24.7 7.9 %collective-permute-done.2 = bf16[128,256]{1,0:T(8,128)(2,1)S(1)} collective-permute-done((bf16[128,256]{1,0:T(8,128)(2,1)S(1)}, bf16[128,256]{1,0:T(8,128)(2,1)S(1)}, u32[]{:S(2)}, u32[]{:S(2)}) %collective-permute-start.2) | collective-permute-done | bytes 65568 | tf_op jit(solution)/shard_map/ppermute | solution.py:95
  32.7 7.9 %collective-permute-done.3 = bf16[128,256]{1,0:T(8,128)(2,1)S(1)} collective-permute-done((bf16[128,256]{1,0:T(8,128)(2,1)S(1)}, bf16[128,256]{1,0:T(8,128)(2,1)S(1)}, u32[]{:S(2)}, u32[]{:S(2)}) %collective-permute-start.3) | collective-permute-done | bytes 65568 | tf_op jit(solution)/shard_map/ppermute | solution.py:95
  44.2 4.5 collective-permute-done.4
  48.7 8.6 %collective-permute-done.5 = bf16[128,256]{1,0:T(8,128)(2,1)S(1)} collective-permute-done((bf16[128,256]{1,0:T(8,128)(2,1)S(1)}, bf16[128,256]{1,0:T(8,128)(2,1)S(1)}, u32[]{:S(2)}, u32[]{:S(2)}) %collective-permute-start.5) | collective-permute-done | bytes 65568 | tf_op jit(solution)/shard_map/ppermute | solution.py:95
  57.2 9.3 %collective-permute-done.6 = bf16[128,256]{1,0:T(8,128)(2,1)S(1)} collective-permute-done((bf16[128,256]{1,0:T(8,128)(2,1)S(1)}, bf16[128,256]{1,0:T(8,128)(2,1)S(1)}, u32[]{:S(2)}, u32[]{:S(2)}) %collective-permute-start.6) | collective-permute-done | bytes 65568 | tf_op jit(solution)/shard_map/ppermute | solution.py:95
  67.3 7.1 %collective-permute-done.7 = bf16[128,256]{1,0:T(8,128)(2,1)S(1)} collective-permute-done((bf16[128,256]{1,0:T(8,128)(2,1)S(1)}, bf16[128,256]{1,0:T(8,128)(2,1)S(1)}, u32[]{:S(2)}, u32[]{:S(2)}) %collective-permute-start.7) | collective-permute-done | bytes 65568 | tf_op jit(solution)/shard_map/ppermute | solution.py:95
  75.1 7.1 %collective-permute-done.8 = bf16[128,256]{1,0:T(8,128)(2,1)S(1)} collective-permute-done((bf16[128,256]{1,0:T(8,128)(2,1)S(1)}, bf16[128,256]{1,0:T(8,128)(2,1)S(1)}, u32[]{:S(2)}, u32[]{:S(2)}) %collective-permute-start.8) | collective-permute-done | bytes 65568 | tf_op jit(solution)/shard_map/ppermute | solution.py:95
  82.2 7.8 %collective-permute-done.9 = bf16[128,256]{1,0:T(8,128)(2,1)S(1)} collective-permute-done((bf16[128,256]{1,0:T(8,128)(2,1)S(1)}, bf16[128,256]{1,0:T(8,128)(2,1)S(1)}, u32[]{:S(2)}, u32[]{:S(2)}) %collective-permute-start.9) | collective-permute-done | bytes 65568 | tf_op jit(solution)/shard_map/ppermute | solution.py:95
  90.2 7.8 %collective-permute-done.10 = bf16[128,256]{1,0:T(8,128)(2,1)S(1)} collective-permute-done((bf16[128,256]{1,0:T(8,128)(2,1)S(1)}, bf16[128,256]{1,0:T(8,128)(2,1)S(1)}, u32[]{:S(2)}, u32[]{:S(2)}) %collective-permute-start.10) | collective-permute-done | bytes 65568 | tf_op jit(solution)/shard_map/ppermute | solution.py:95
  98.0 7.8 %collective-permute-done.11 = bf16[128,256]{1,0:T(8,128)(2,1)S(1)} collective-permute-done((bf16[128,256]{1,0:T(8,128)(2,1)S(1)}, bf16[128,256]{1,0:T(8,128)(2,1)S(1)}, u32[]{:S(2)}, u32[]{:S(2)}) %collective-permute-start.11) | collective-permute-done | bytes 65568 | tf_op jit(solution)/shard_map/ppermute | solution.py:95
  105.9 8.4 %collective-permute-done.12 = bf16[128,256]{1,0:T(8,128)(2,1)} collective-permute-done((bf16[128,256]{1,0:T(8,128)(2,1)S(1)}, bf16[128,256]{1,0:T(8,128)(2,1)}, u32[]{:S(2)}, u32[]{:S(2)}) %collective-permute-start.12) | collective-permute-done | bytes 65568 | tf_op jit(solution)/shard_map/ppermute | solution.py:95
  115.4 7.1 %collective-permute-done.13 = bf16[128,256]{1,0:T(8,128)(2,1)} collective-permute-done((bf16[128,256]{1,0:T(8,128)(2,1)}, bf16[128,256]{1,0:T(8,128)(2,1)}, u32[]{:S(2)}, u32[]{:S(2)}) %collective-permute-start.13) | collective-permute-done | bytes 65568 | tf_op jit(solution)/shard_map/ppermute | solution.py:95
  123.3 7.3 %collective-permute-done.14 = bf16[128,256]{1,0:T(8,128)(2,1)S(1)} collective-permute-done((bf16[128,256]{1,0:T(8,128)(2,1)}, bf16[128,256]{1,0:T(8,128)(2,1)S(1)}, u32[]{:S(2)}, u32[]{:S(2)}) %collective-permute-start.14) | collective-permute-done | bytes 65568 | tf_op jit(solution)/shard_map/ppermute | solution.py:95
  146.8 7.3 %fusion.57 = (f32[4,256]{1,0:T(4,128)S(1)}, f32[4,256,2048]{2,1,0:T(8,128)S(1)}) fusion(f32[2048,4,32]{0,2,1:T(8,128)S(1)} %get-tuple-element.18, f32[2048,4,32]{0,2,1:T(8,128)S(1)} %get-tuple-element.17, f32[4,2,8,8,128]{4,3,2,1,0:T(8,128)S(1)} %bitcast.37), kind=kOutput, calls=%fused_computation.140 | convolution fusion | flops 1613233152 | bytes 10752000 | tf_op jit(solution)/shard_map/while/body/eval_jaxpr/hrd,shd->hrs/dot_general | solution.py:145
  166.8 130.9 %all-gather.9.cloned.1.call-done = bf16[2048,2560]{1,0:T(8,128)(2,1)} async-done(((bf16[128,2560]{1,0:T(8,128)(2,1)}), bf16[2048,2560]{1,0:T(8,128)(2,1)}) %all-gather.9.cloned.1.call-update) | async-done | bytes 10485776 | tf_op jit(solution)/shard_map/all_gather | solution.py:108
  297.7 5.5 convolution_convert_fusion
  303.2 126.7 %all-gather.7.cloned.1.call-done = bf16[2048,2560]{1,0:T(8,128)(2,1)} async-done(((bf16[128,2560]{1,0:T(8,128)(2,1)}), bf16[2048,2560]{1,0:T(8,128)(2,1)}) %all-gather.7.cloned.1.call-update) | async-done | bytes 10485776 | tf_op jit(solution)/shard_map/all_gather | solution.py:107
  429.9 5.5 convolution_convert_fusion.1
  440.5 4.6 collective-permute-done.16
  447.8 114.3 %all-gather.11.cloned.1.call-done = bf16[2048,2560]{1,0:T(8,128)(2,1)} async-done(((bf16[128,2560]{1,0:T(8,128)(2,1)}), bf16[2048,2560]{1,0:T(8,128)(2,1)}) %all-gather.11.cloned.1.call-update) | async-done | bytes 10485776 | tf_op jit(solution)/shard_map/all_gather | solution.py:109
  562.1 9.2 %convolution_convert_fusion.3 = bf16[128,2048]{1,0:T(8,128)(2,1)} fusion(bf16[2048,2560]{1,0:T(8,128)(2,1)} %all-gather.11.cloned.1.call-done, f32[128,5120]{1,0:T(8,128)} %fusion.5), kind=kOutput, calls=%fused_computation.13 | convolution fusion | flops 1344405504 | bytes 13631488 | tf_op jit(solution)/shard_map/dot_general | solution.py:69
  571.3 6.3 %reduce-scatter.5.cloned.1.call-done = bf16[64,2048]{1,0:T(8,128)(2,1)} async-done(((bf16[128,2048]{1,0:T(8,128)(2,1)}), bf16[64,2048]{1,0:T(8,128)(2,1)}) %reduce-scatter.5.cloned.1.call-update) | async-done | bytes 262160 | tf_op jit(solution)/shard_map/reduce_scatter | solution.py:192
  (147 shorter events, 51.1 us)
Async XLA Ops:
  6.5 150.5 %copy-start = (bf16[512,2048]{1,0:T(8,128)(2,1)S(1)}, bf16[512,2048]{1,0:T(8,128)(2,1)}, u32[]{:S(2)}) copy-start(bf16[512,2048]{1,0:T(8,128)(2,1)} %param.19) | copy-start | bytes 6291460
  6.5 133.0 %all-gather.5.cloned.1.call-start = ((), (), s32[]{:S(2)}) async-start(), calls=%async_computation.2 | async-start | bytes 1114112 | tf_op jit(solution)/shard_map/all_gather | solution.py:130
  7.3 155.1 %reduce-scatter.3.cloned.1.call-start = ((), (), s32[]{:S(2)}) async-start(), calls=%async_computation.3 | async-start | bytes 786432 | tf_op jit(solution)/shard_map/reduce_scatter | solution.py:169
  7.3 9.5 %collective-permute-start = (bf16[128,256]{1,0:T(8,128)(2,1)}, bf16[128,256]{1,0:T(8,128)(2,1)S(1)}, u32[]{:S(2)}, u32[]{:S(2)}) collective-permute-start(bf16[128,256]{1,0:T(8,128)(2,1)} %param.16), channel_id=1, source_target_pairs={{0,2},{2,4},{4,6},{6,8},{8,10},{10,12},{12,14},{14,16},{16,18},{18... | collective-permute-start | bytes 196616 | tf_op jit(solution)/shard_map/ppermute | solution.py:95
  16.8 7.9 %collective-permute-start.1 = (bf16[128,256]{1,0:T(8,128)(2,1)S(1)}, bf16[128,256]{1,0:T(8,128)(2,1)S(1)}, u32[]{:S(2)}, u32[]{:S(2)}) collective-permute-start(bf16[128,256]{1,0:T(8,128)(2,1)S(1)} %collective-permute-done), channel_id=1, source_target_pairs={{0,2},{2,4},{4,6},{6,8},{8,10},{10,12},{12,14},{14,16},{16,18},{18... | collective-permute-start | bytes 196616 | tf_op jit(solution)/shard_map/ppermute | solution.py:95
  24.7 7.9 %collective-permute-start.2 = (bf16[128,256]{1,0:T(8,128)(2,1)S(1)}, bf16[128,256]{1,0:T(8,128)(2,1)S(1)}, u32[]{:S(2)}, u32[]{:S(2)}) collective-permute-start(bf16[128,256]{1,0:T(8,128)(2,1)S(1)} %collective-permute-done.1), channel_id=1, source_target_pairs={{0,2},{2,4},{4,6},{6,8},{8,10},{10,12},{12,14},{14,16},{16,18},{18... | collective-permute-start | bytes 196616 | tf_op jit(solution)/shard_map/ppermute | solution.py:95
  32.6 8.0 %collective-permute-start.3 = (bf16[128,256]{1,0:T(8,128)(2,1)S(1)}, bf16[128,256]{1,0:T(8,128)(2,1)S(1)}, u32[]{:S(2)}, u32[]{:S(2)}) collective-permute-start(bf16[128,256]{1,0:T(8,128)(2,1)S(1)} %collective-permute-done.2), channel_id=1, source_target_pairs={{0,2},{2,4},{4,6},{6,8},{8,10},{10,12},{12,14},{14,16},{16,18},{18... | collective-permute-start | bytes 196616 | tf_op jit(solution)/shard_map/ppermute | solution.py:95
  40.6 8.0 %collective-permute-start.4 = (bf16[128,256]{1,0:T(8,128)(2,1)S(1)}, bf16[128,256]{1,0:T(8,128)(2,1)S(1)}, u32[]{:S(2)}, u32[]{:S(2)}) collective-permute-start(bf16[128,256]{1,0:T(8,128)(2,1)S(1)} %collective-permute-done.3), channel_id=1, source_target_pairs={{0,2},{2,4},{4,6},{6,8},{8,10},{10,12},{12,14},{14,16},{16,18},{18... | collective-permute-start | bytes 196616 | tf_op jit(solution)/shard_map/ppermute | solution.py:95
  48.6 8.6 %collective-permute-start.5 = (bf16[128,256]{1,0:T(8,128)(2,1)S(1)}, bf16[128,256]{1,0:T(8,128)(2,1)S(1)}, u32[]{:S(2)}, u32[]{:S(2)}) collective-permute-start(bf16[128,256]{1,0:T(8,128)(2,1)S(1)} %collective-permute-done.4), channel_id=1, source_target_pairs={{0,2},{2,4},{4,6},{6,8},{8,10},{10,12},{12,14},{14,16},{16,18},{18... | collective-permute-start | bytes 196616 | tf_op jit(solution)/shard_map/ppermute | solution.py:95
  57.2 9.3 %collective-permute-start.6 = (bf16[128,256]{1,0:T(8,128)(2,1)S(1)}, bf16[128,256]{1,0:T(8,128)(2,1)S(1)}, u32[]{:S(2)}, u32[]{:S(2)}) collective-permute-start(bf16[128,256]{1,0:T(8,128)(2,1)S(1)} %collective-permute-done.5), channel_id=1, source_target_pairs={{0,2},{2,4},{4,6},{6,8},{8,10},{10,12},{12,14},{14,16},{16,18},{18... | collective-permute-start | bytes 196616 | tf_op jit(solution)/shard_map/ppermute | solution.py:95
  66.5 7.9 %collective-permute-start.7 = (bf16[128,256]{1,0:T(8,128)(2,1)S(1)}, bf16[128,256]{1,0:T(8,128)(2,1)S(1)}, u32[]{:S(2)}, u32[]{:S(2)}) collective-permute-start(bf16[128,256]{1,0:T(8,128)(2,1)S(1)} %collective-permute-done.6), channel_id=1, source_target_pairs={{0,2},{2,4},{4,6},{6,8},{8,10},{10,12},{12,14},{14,16},{16,18},{18... | collective-permute-start | bytes 196616 | tf_op jit(solution)/shard_map/ppermute | solution.py:95
  74.4 7.9 %collective-permute-start.8 = (bf16[128,256]{1,0:T(8,128)(2,1)S(1)}, bf16[128,256]{1,0:T(8,128)(2,1)S(1)}, u32[]{:S(2)}, u32[]{:S(2)}) collective-permute-start(bf16[128,256]{1,0:T(8,128)(2,1)S(1)} %collective-permute-done.7), channel_id=1, source_target_pairs={{0,2},{2,4},{4,6},{6,8},{8,10},{10,12},{12,14},{14,16},{16,18},{18... | collective-permute-start | bytes 196616 | tf_op jit(solution)/shard_map/ppermute | solution.py:95
  82.2 7.9 %collective-permute-start.9 = (bf16[128,256]{1,0:T(8,128)(2,1)S(1)}, bf16[128,256]{1,0:T(8,128)(2,1)S(1)}, u32[]{:S(2)}, u32[]{:S(2)}) collective-permute-start(bf16[128,256]{1,0:T(8,128)(2,1)S(1)} %collective-permute-done.8), channel_id=1, source_target_pairs={{0,2},{2,4},{4,6},{6,8},{8,10},{10,12},{12,14},{14,16},{16,18},{18... | collective-permute-start | bytes 196616 | tf_op jit(solution)/shard_map/ppermute | solution.py:95
  90.1 7.9 %collective-permute-start.10 = (bf16[128,256]{1,0:T(8,128)(2,1)S(1)}, bf16[128,256]{1,0:T(8,128)(2,1)S(1)}, u32[]{:S(2)}, u32[]{:S(2)}) collective-permute-start(bf16[128,256]{1,0:T(8,128)(2,1)S(1)} %collective-permute-done.9), channel_id=1, source_target_pairs={{0,2},{2,4},{4,6},{6,8},{8,10},{10,12},{12,14},{14,16},{16,18},{18... | collective-permute-start | bytes 196616 | tf_op jit(solution)/shard_map/ppermute | solution.py:95
  98.0 7.9 %collective-permute-start.11 = (bf16[128,256]{1,0:T(8,128)(2,1)S(1)}, bf16[128,256]{1,0:T(8,128)(2,1)S(1)}, u32[]{:S(2)}, u32[]{:S(2)}) collective-permute-start(bf16[128,256]{1,0:T(8,128)(2,1)S(1)} %collective-permute-done.10), channel_id=1, source_target_pairs={{0,2},{2,4},{4,6},{6,8},{8,10},{10,12},{12,14},{14,16},{16,18},{18... | collective-permute-start | bytes 196616 | tf_op jit(solution)/shard_map/ppermute | solution.py:95
  105.9 8.5 %collective-permute-start.12 = (bf16[128,256]{1,0:T(8,128)(2,1)S(1)}, bf16[128,256]{1,0:T(8,128)(2,1)}, u32[]{:S(2)}, u32[]{:S(2)}) collective-permute-start(bf16[128,256]{1,0:T(8,128)(2,1)S(1)} %collective-permute-done.11), channel_id=1, source_target_pairs={{0,2},{2,4},{4,6},{6,8},{8,10},{10,12},{12,14},{14,16},{16,18},{18... | collective-permute-start | bytes 196616 | tf_op jit(solution)/shard_map/ppermute | solution.py:95
  114.4 8.2 %collective-permute-start.13 = (bf16[128,256]{1,0:T(8,128)(2,1)}, bf16[128,256]{1,0:T(8,128)(2,1)}, u32[]{:S(2)}, u32[]{:S(2)}) collective-permute-start(bf16[128,256]{1,0:T(8,128)(2,1)} %collective-permute-done.12), channel_id=1, source_target_pairs={{0,2},{2,4},{4,6},{6,8},{8,10},{10,12},{12,14},{14,16},{16,18},{18... | collective-permute-start | bytes 196616 | tf_op jit(solution)/shard_map/ppermute | solution.py:95
  122.5 8.1 %collective-permute-start.14 = (bf16[128,256]{1,0:T(8,128)(2,1)}, bf16[128,256]{1,0:T(8,128)(2,1)S(1)}, u32[]{:S(2)}, u32[]{:S(2)}) collective-permute-start(bf16[128,256]{1,0:T(8,128)(2,1)} %collective-permute-done.13), channel_id=1, source_target_pairs={{0,2},{2,4},{4,6},{6,8},{8,10},{10,12},{12,14},{14,16},{16,18},{18... | collective-permute-start | bytes 196616 | tf_op jit(solution)/shard_map/ppermute | solution.py:95
  158.4 139.3 %all-gather.9.cloned.1.call-start = ((), (), s32[]{:S(2)}) async-start(), calls=%async_computation.5 | async-start | bytes 11141120 | tf_op jit(solution)/shard_map/all_gather | solution.py:108
  159.1 270.8 %all-gather.7.cloned.1.call-start = ((), (), s32[]{:S(2)}) async-start(), calls=%async_computation.4 | async-start | bytes 11141120 | tf_op jit(solution)/shard_map/all_gather | solution.py:107
  159.7 402.4 %all-gather.11.cloned.1.call-start = ((), (), s32[]{:S(2)}) async-start(), calls=%async_computation.6 | async-start | bytes 11141120 | tf_op jit(solution)/shard_map/all_gather | solution.py:109
  160.3 417.3 %reduce-scatter.5.cloned.1.call-start = ((), (), s32[]{:S(2)}) async-start(), calls=%async_computation.7 | async-start | bytes 786432 | tf_op jit(solution)/shard_map/reduce_scatter | solution.py:192
  435.5 5.0 collective-permute-start.15
  438.8 6.2 %collective-permute-start.16 = (bf16[1,5120]{1,0:T(2,128)(2,1)S(1)}, bf16[1,5120]{1,0:T(2,128)(2,1)S(1)}, u32[]{:S(2)}, u32[]{:S(2)}) collective-permute-start(bf16[1,5120]{1,0:T(2,128)(2,1)S(1)} %get-tuple-element.33), channel_id=1, source_target_pairs={{2,0},{4,2},{6,4},{8,6},{10,8},{12,10},{14,12},{16,14},{18,16},{20... | collective-permute-start | bytes 30728 | tf_op jit(solution)/shard_map/ppermute | solution.py:23
  (19 other events, 358.5 us)
Sparse Core Ops, SparseCore 0:
  10.1 59.4 all-gather.4
  158.5 3.7 reduce-scatter.2
  165.1 132.5 all-gather.8
  300.2 129.6 all-gather.6
  432.4 129.6 all-gather.10
  571.5 6.0 reduce-scatter.4
